TPU v7x, 32 devices: a whole 2x2x4 slice. The times are simulated.
32 devices in a mesh: grp: 2 (over y), ep: 4 (over z), tp: 4 (over x, core).
Axes of the slice: x: 2, y: 2, z: 4, core: 2. Of those that a mesh axis runs over, the one named last changes fastest.
Arguments:
- query_rows: bfloat16 [1536, 2048], P(('grp', 'ep'), 'tp'), parts along dimension 0, may hold values from -100 to 100
- projected_keys: bfloat16 [1536, 512], P(('grp', 'ep'), 'tp'), parts along dimension 0, may hold values from -100 to 100
- projected_values: bfloat16 [1536, 512], P(('grp', 'ep'), 'tp'), parts along dimension 0, may hold values from -6 to 6
- query_gain: float32 [128], replicated, may hold values from 0.3 to 6.5
- key_norm_gain: float32 [128], replicated, may hold values from 0.3 to 6.5
- out_proj: bfloat16 [2048, 2048], P('tp'), may hold values from -4 to 4
- mix_tokens: bfloat16 [4096, 2048], P(('grp', 'ep', 'tp')), parts along dimension 0, may hold values from -150 to 150
- norm_gain: float32 [2048], replicated, may hold values from 0.1 to 1.9
- expert_ids: int32 [4096, 2], P(('grp', 'ep', 'tp')), parts along dimension 0, may hold values from 0 to 3, all different within a row; in each aligned block of 128 rows (0 to 127, 128 to 255, ...) at most 96 rows name the same one
- expert_score: float32 [4096, 2], P(('grp', 'ep', 'tp')), parts along dimension 0, may hold values from -6 to 6
- gate_proj: bfloat16 [4, 2048, 2048], P('ep', None, 'tp'), may hold values from -0.125 to 0.125
- up_proj: bfloat16 [4, 2048, 2048], P('ep', None, 'tp'), may hold values from -0.125 to 0.125
- down_proj: bfloat16 [4, 2048, 2048], P('ep', 'tp'), may hold values from -0.125 to 0.125
Outputs:
- mixed_rows: bfloat16 [1536, 2048], P(('grp', 'ep', 'tp')), parts along dimension 0
- expert_out: bfloat16 [4096, 2048], P(('grp', 'ep', 'tp')), parts along dimension 0
There are 2 independent parts, one for each index of `grp`. A program takes and returns all parts, laid end to end along the dimension named above; an argument that names none is the same for every part. Nothing has to cross between parts.
Inputs may be any that keep to these rules, and one draw needn't show every extreme that they name: `expert_ids`: each row names 2 different experts. Within the rows of one device (aligned blocks of 128 rows) no expert is named more than 96 times, and in every draw some device names some expert exactly 96 times.
All inputs are finite; a program needn't handle non-finite values.
Results may differ from a plain program's by a relative error of at most 0.014.
The roundings to bfloat16 on the way count: a program that leaves them out, or rounds other values in their place, can miss the bound.
Values may be sent and summed in bfloat16 or wider, within the bound.
A program may use at most 128 MiB of HBM per device.

v0:
```python
import math
import jax
import jax.numpy as jnp
from jax import lax
from jax.sharding import PartitionSpec as P

GRID_W = 64
EPS = 1e-06
THETA = 10000.0


def head_norm(vectors, gain):
    return vectors * lax.rsqrt(jnp.mean(vectors * vectors, axis=-1, keepdims=True) + EPS) * gain


def rotate_grid(vectors, token_positions):
    length, heads, head_dim = vectors.shape
    quarter = head_dim // 4
    freqs = 1.0 / THETA ** (jnp.arange(quarter, dtype=jnp.float32) * 4.0 / head_dim)
    grid_row = (token_positions // GRID_W).astype(jnp.float32)
    grid_col = (token_positions % GRID_W).astype(jnp.float32)
    angles = jnp.stack([grid_row[:, None] * freqs, grid_col[:, None] * freqs], axis=1)
    cosine = jnp.cos(angles)[:, None]
    sine = jnp.sin(angles)[:, None]
    halves = vectors.reshape(length, heads, 2, 2, quarter)
    first = halves[..., 0, :]
    second = halves[..., 1, :]
    turned = jnp.stack([first * cosine - second * sine, second * cosine + first * sine], axis=-2)
    return turned.reshape(length, heads, head_dim)


def prepare_inputs(raw_rows, gain, heads, token_positions):
    length = raw_rows.shape[0]
    head_dim = gain.shape[0]
    vectors = raw_rows.astype(jnp.float32).reshape(length, heads, head_dim)
    return rotate_grid(head_norm(vectors, gain), token_positions).astype(jnp.bfloat16)


def mixer_half(query_rows, projected_keys, projected_values, query_gain, key_norm_gain, out_proj):
    length = query_rows.shape[0]
    head_dim = query_gain.shape[0]
    kv_heads = projected_keys.shape[1] // head_dim
    q_heads = query_rows.shape[1] // head_dim
    queries_per_group = q_heads // kv_heads
    token_positions = lax.axis_index("ep") * length + jnp.arange(length, dtype=jnp.int32)
    query_matrix = prepare_inputs(query_rows, query_gain, q_heads, token_positions).reshape(
        length, kv_heads, queries_per_group, head_dim
    )
    keys_turned = prepare_inputs(projected_keys, key_norm_gain, kv_heads, token_positions).reshape(
        length, kv_heads * head_dim
    )
    score_scale = head_dim ** (-0.5)
    initial = (
        jnp.full((kv_heads, queries_per_group, length), -1e30, jnp.float32),
        jnp.zeros((kv_heads, queries_per_group, length), jnp.float32),
        jnp.zeros((length, kv_heads, queries_per_group, head_dim), jnp.float32),
    )
    key_piece = lax.all_gather(keys_turned, "ep", axis=0, tiled=True)
    value_piece = lax.all_gather(projected_values, "ep", axis=0, tiled=True)
    piece_rows = key_piece.shape[0]
    step_rows = math.gcd(piece_rows, 1024)

    def one_block(block_index, running):
        run_max, run_sum, run_acc = running
        offset = block_index * step_rows
        key_block = lax.dynamic_slice_in_dim(key_piece, offset, step_rows, 0).reshape(
            step_rows, kv_heads, head_dim
        )
        value_block = lax.dynamic_slice_in_dim(value_piece, offset, step_rows, 0).reshape(
            step_rows, kv_heads, head_dim
        )
        scores = (
            jnp.einsum(
                "tkgd,skd->kgts", query_matrix, key_block, preferred_element_type=jnp.float32
            )
            * score_scale
        )
        new_max = jnp.maximum(run_max, jnp.max(scores, axis=-1))
        factor = jnp.exp(run_max - new_max)
        weights = jnp.exp(scores - new_max[..., None])
        run_sum = run_sum * factor + jnp.sum(weights, axis=-1)
        update = jnp.einsum(
            "kgts,skd->tkgd",
            weights.astype(jnp.bfloat16),
            value_block,
            preferred_element_type=jnp.float32,
        )
        run_acc = run_acc * jnp.transpose(factor, (2, 0, 1))[..., None] + update
        return (new_max, run_sum, run_acc)

    run_max, run_sum, run_acc = lax.fori_loop(0, piece_rows // step_rows, one_block, initial)
    heads_out = (
        (run_acc / jnp.transpose(run_sum, (2, 0, 1))[..., None])
        .astype(jnp.bfloat16)
        .reshape(length, q_heads * head_dim)
    )
    return lax.psum_scatter(
        jnp.dot(heads_out, out_proj, preferred_element_type=jnp.float32).astype(jnp.bfloat16),
        "tp",
        scatter_dimension=0,
        tiled=True,
    )


def expert_half(mix_tokens, norm_gain, expert_ids, expert_score, gate_proj, up_proj, down_proj):
    length, model_dim = mix_tokens.shape
    top_count = expert_ids.shape[1]
    local_experts = gate_proj.shape[0]
    expert_axis = lax.axis_size("ep")
    experts_all = expert_axis * local_experts
    capacity = length * top_count * 3 // (2 * experts_all)
    values_b = mix_tokens.astype(jnp.float32)
    normed = (
        values_b
        * lax.rsqrt(jnp.mean(values_b * values_b, axis=-1, keepdims=True) + EPS)
        * norm_gain
    ).astype(jnp.bfloat16)
    flat = expert_ids.reshape(length * top_count)
    onehot = (flat[:, None] == jnp.arange(experts_all, dtype=jnp.int32)).astype(jnp.int32)
    slots = jnp.sum((jnp.cumsum(onehot, axis=0) - onehot) * onehot, axis=1)
    target = flat * capacity + slots
    placed = (target[:, None] == jnp.arange(experts_all * capacity, dtype=jnp.int32)).astype(
        jnp.int32
    )
    placed = jnp.sum(placed.reshape(length, top_count, experts_all * capacity), axis=1).astype(
        jnp.bfloat16
    )
    outgoing = jnp.einsum("re,rd->ed", placed, normed, preferred_element_type=jnp.float32).astype(
        jnp.bfloat16
    )
    outgoing = outgoing.reshape(expert_axis, local_experts, capacity, model_dim)
    rows_in = lax.all_gather(
        lax.all_to_all(outgoing, "ep", split_axis=0, concat_axis=0, tiled=True),
        "tp",
        axis=0,
        tiled=True,
    )
    gate_out = jnp.einsum("secd,edf->secf", rows_in, gate_proj, preferred_element_type=jnp.float32)
    up_out = jnp.einsum("secd,edf->secf", rows_in, up_proj, preferred_element_type=jnp.float32)
    active = (jax.nn.silu(gate_out) * up_out).astype(jnp.bfloat16)
    summed = lax.psum_scatter(
        jnp.einsum("secf,efd->secd", active, down_proj, preferred_element_type=jnp.float32).astype(
            jnp.bfloat16
        ),
        "tp",
        scatter_dimension=0,
        tiled=True,
    )
    returned = lax.all_to_all(summed, "ep", split_axis=0, concat_axis=0, tiled=True)
    results = returned.reshape(experts_all * capacity, model_dim)
    selected_expert = target.reshape(length, top_count)
    first_weight = jax.nn.sigmoid(expert_score[:, 0] - expert_score[:, 1])
    combined = first_weight[:, None] * results[selected_expert[:, 0]].astype(jnp.float32) + (
        1.0 - first_weight
    )[:, None] * results[selected_expert[:, 1]].astype(jnp.float32)
    return combined.astype(jnp.bfloat16)


def local(
    query_rows,
    projected_keys,
    projected_values,
    query_gain,
    key_norm_gain,
    out_proj,
    mix_tokens,
    norm_gain,
    expert_ids,
    expert_score,
    gate_proj,
    up_proj,
    down_proj,
):
    mixed_rows = mixer_half(
        query_rows, projected_keys, projected_values, query_gain, key_norm_gain, out_proj
    )
    expert_out = expert_half(
        mix_tokens, norm_gain, expert_ids, expert_score, gate_proj, up_proj, down_proj
    )
    return (mixed_rows, expert_out)


def solution(mesh):
    in_specs = (
        P(("grp", "ep"), "tp"),
        P(("grp", "ep"), "tp"),
        P(("grp", "ep"), "tp"),
        P(),
        P(),
        P("tp", None),
        P(("grp", "ep", "tp"), None),
        P(),
        P(("grp", "ep", "tp"), None),
        P(("grp", "ep", "tp"), None),
        P("ep", None, "tp"),
        P("ep", None, "tp"),
        P("ep", "tp", None),
    )
    out_specs = (P(("grp", "ep", "tp"), None), P(("grp", "ep", "tp"), None))
    return jax.shard_map(local, mesh=mesh, in_specs=in_specs, out_specs=out_specs, check_vma=False)
```

profile of v0, /device:TPU:0, one launch (start us, length us, event | category | flops | bytes accessed | tf_op | source)
XLA Modules:
  0.0 237.6 jit_solution(8891725918785150637)
XLA Ops:
  7.2 0.9 copy.76
  8.4 1.2 reduce-window.6
  10.3 0.7 multiply_add_fusion
  11.1 1.2 fusion.39
  12.3 1.7 convolution_convert_fusion
  14.1 43.2 %all_to_all.10 = bf16[4,1,96,2048]{3,2,1,0:T(8,128)(2,1)} all-to-all(bf16[4,1,96,2048]{3,2,1,0:T(8,128)(2,1)S(1)} %bitcast.175), channel_id=1, replica_groups=mesh['grp'=2,'ep'=4,'tp'=4] {'ep'}, dimensions={0} | all-to-all | bytes 3145728 | tf_op jit(solution)/shard_map/all_to_all | solution.py:133
  57.4 45.6 %all-gather.2.cloned.1.call-done = bf16[16,1,96,2048]{3,2,1,0:T(8,128)(2,1)} async-done(((bf16[4,1,96,2048]{3,2,1,0:T(8,128)(2,1)}), bf16[16,1,96,2048]{3,2,1,0:T(8,128)(2,1)}) %all-gather.2.cloned.1.call-update) | async-done | bytes 6291472 | tf_op jit(solution)/shard_map/all_gather | solution.py:132
  103.0 8.5 %fusion.15 = f32[16,96,512]{2,1,0:T(8,128)} fusion(bf16[16,1,96,2048]{3,2,1,0:T(8,128)(2,1)} %all-gather.2.cloned.1.call-done, bf16[1,2048,512]{2,1,0:T(8,128)(2,1)} %param.26), kind=kOutput, calls=%fused_computation.24 | convolution fusion | flops 3221225472 | bytes 11534336 | tf_op jit(solution)/shard_map/secd,edf->secf/dot_general | solution.py:139
  111.5 11.9 %convert_bitcast_fusion = bf16[16,1,96,2048]{3,2,0,1:T(8,128)(2,1)} fusion(bf16[1,512,2048]{2,1,0:T(8,128)(2,1)S(1)} %copy-done, f32[16,96,512]{2,1,0:T(8,128)} %fusion.15, bf16[1,2048,512]{2,1,0:T(8,128)(2,1)} %param.25, bf16[16,1,96,2048]{3,2,1,0:T(8,128)(2,1)} %all-gather.2.cloned.1.call-done), kind=kOutput, calls=%fused_computation.28 | convolution fusion | flops 6450315264 | bytes 19922944 | tf_op jit(solution)/shard_map/secf,efd->secd/dot_general | solution.py:142
  123.5 0.8 copy-done.1
  124.7 0.2 fusion.51
  125.7 0.3 subtract_convert_fusion.1
  126.1 14.4 %all_gather.9 = bf16[768,128]{1,0:T(8,128)(2,1)} all-gather(bf16[192,128]{1,0:T(8,128)(2,1)S(1)} %copy.72), channel_id=1, replica_groups=mesh['grp'=2,'ep'=4,'tp'=4] {'ep'}, dimensions={0}, use_global_device_ids=true | all-gather | bytes 245760 | tf_op jit(solution)/shard_map/all_gather | solution.py:58
  140.5 14.8 %all_gather.10 = bf16[768,128]{1,0:T(8,128)(2,1)} all-gather(bf16[192,128]{1,0:T(8,128)(2,1)S(1)} %copy-done.3), channel_id=1, replica_groups=mesh['grp'=2,'ep'=4,'tp'=4] {'ep'}, dimensions={0}, use_global_device_ids=true | all-gather | bytes 245760 | tf_op jit(solution)/shard_map/all_gather | solution.py:59
  155.2 27.2 %reduce-scatter.5.cloned.1.call-done = bf16[4,1,96,2048]{3,2,0,1:T(8,128)(2,1)} async-done(((bf16[16,1,96,2048]{3,2,0,1:T(8,128)(2,1)}), bf16[4,1,96,2048]{3,2,0,1:T(8,128)(2,1)}) %reduce-scatter.5.cloned.1.call-update) | async-done | bytes 1572880 | tf_op jit(solution)/shard_map/reduce_scatter | solution.py:141
  182.4 4.6 %all-to-all-start.1 = ((bf16[4,1,96,2048]{3,2,1,0:T(8,128)(2,1)}), bf16[4,1,96,2048]{3,2,1,0:T(8,128)(2,1)}, u32[]{:S(2)}, u32[]{:S(2)}) async-start(bf16[4,1,96,2048]{3,2,1,0:T(8,128)(2,1)} %bitcast.179), calls=%async_computation.3 | async-start | bytes 3145728 | tf_op jit(solution)/shard_map/all_to_all | solution.py:149
  187.0 8.8 %while.18 = (s32[]{:T(128)}, f32[1,4,192]{2,1,0:T(4,128)S(1)}, f32[1,4,192]{2,1,0:T(4,128)S(1)}, f32[192,1,4,128]{3,0,2,1:T(8,128)S(1)}, bf16[768,128]{1,0:T(8,1...) while((s32[]{:T(128)}, f32[1,4,192]{2,1,0:T(4,128)S(1)}, ...), condition=%wide.region_5.6_spmd.clone, body=%wide.region_2.5_spmd.clone.sunk | while | flops 102142472 | bytes 3522735 | solution.py:91
  187.0 1.2 fusion.75
  188.3 1.2 fusion.78
  189.5 0.4 fusion.77
  189.9 1.3 fusion.75
  191.2 1.2 fusion.78
  192.5 0.4 fusion.77
  192.9 1.3 fusion.75
  194.2 1.2 fusion.78
  195.4 0.4 fusion.77
  195.8 0.2 divide_convert_fusion
  196.2 3.1 %convolution_convert_fusion.1 = bf16[192,2048]{1,0:T(8,128)(2,1)} fusion(bf16[512,2048]{1,0:T(8,128)(2,1)} %param.20, bf16[24,8,4,128]{3,2,1,0:T(4,128)(2,1)S(1)} %bitcast.181), kind=kOutput, calls=%fused_computation.37 | convolution fusion | flops 403046400 | bytes 3080192 | tf_op jit(solution)/shard_map/dot_general | solution.py:98
  199.3 24.6 %all-to-all-done.1 = bf16[4,1,96,2048]{3,2,1,0:T(8,128)(2,1)} async-done(((bf16[4,1,96,2048]{3,2,1,0:T(8,128)(2,1)}), bf16[4,1,96,2048]{3,2,1,0:T(8,128)(2,1)}, u32[]{:S(2)}, u32[]{:S(2)}) %all-to-all-start.1) | async-done | bytes 1572896 | tf_op jit(solution)/shard_map/all_to_all | solution.py:149
  223.9 3.0 %gather_fusion = bf16[128,2048]{1,0:T(8,128)(2,1)S(1)} fusion(bf16[384,2048]{1,0:T(8,128)(2,1)} %bitcast.34, s32[1024]{0:T(1024)S(1)} %get-tuple-element.225), kind=kCustom, calls=%fused_computation | custom fusion | bytes 1049088 | tf_op jit(solution)/shard_map/gather | solution.py:153
  227.0 3.1 %gather_fusion.1 = bf16[128,2048]{1,0:T(8,128)(2,1)S(1)} fusion(bf16[384,2048]{1,0:T(8,128)(2,1)} %bitcast.34, s32[1024]{0:T(1024)S(1)} %get-tuple-element.224), kind=kCustom, calls=%fused_computation.1 | custom fusion | bytes 1049088 | tf_op jit(solution)/shard_map/gather | solution.py:155
  230.0 1.0 add_convert_fusion
  (67 shorter events, 2.6 us)
Async XLA Ops:
  7.2 104.3 %copy-start = (bf16[1,512,2048]{2,1,0:T(8,128)(2,1)S(1)}, bf16[1,512,2048]{2,1,0:T(8,128)(2,1)}, u32[]{:S(2)}) copy-start(bf16[1,512,2048]{2,1,0:T(8,128)(2,1)} %param.27) | copy-start | bytes 6291460
  7.2 95.8 %all-gather.2.cloned.1.call-start = ((), (), s32[]{:S(2)}) async-start(), calls=%async_computation.5 | async-start | bytes 7864320 | tf_op jit(solution)/shard_map/all_gather | solution.py:132
  57.3 125.1 %reduce-scatter.5.cloned.1.call-start = ((), (), s32[]{:S(2)}) async-start(), calls=%async_computation.6 | async-start | bytes 7864320 | tf_op jit(solution)/shard_map/reduce_scatter | solution.py:141
  123.4 0.9 copy-start.1
  123.4 1.1 copy-start.6
  123.4 2.0 copy-start.2
  123.4 2.2 copy-start.5
  124.9 15.6 %copy-start.3 = (bf16[192,128]{1,0:T(8,128)(2,1)S(1)}, bf16[192,128]{1,0:T(8,128)(2,1)}, u32[]{:S(2)}) copy-start(bf16[192,128]{1,0:T(8,128)(2,1)} %param.17) | copy-start | bytes 147460
  182.4 41.5 %all-to-all-start.1 = ((bf16[4,1,96,2048]{3,2,1,0:T(8,128)(2,1)}), bf16[4,1,96,2048]{3,2,1,0:T(8,128)(2,1)}, u32[]{:S(2)}, u32[]{:S(2)}) async-start(bf16[4,1,96,2048]{3,2,1,0:T(8,128)(2,1)} %bitcast.179), calls=%async_computation.3 | async-start | bytes 3145728 | tf_op jit(solution)/shard_map/all_to_all | solution.py:149
  187.0 44.1 %reduce-scatter.3.cloned.1.call-start = ((), (), s32[]{:S(2)}) async-start(), calls=%async_computation.4 | async-start | bytes 983040 | tf_op jit(solution)/shard_map/reduce_scatter | solution.py:97
  196.0 3.3 %copy-start.4 = (f32[128,2]{0,1:T(2,128)S(1)}, f32[128,2]{0,1:T(2,128)}, u32[]{:S(2)}) copy-start(f32[128,2]{0,1:T(2,128)} %param.24) | copy-start | bytes 3076
Sparse Core Ops, SparseCore 0:
  57.4 45.4 all-gather.1
  123.5 58.8 reduce-scatter.4
  199.4 23.6 reduce-scatter.2
where the time goes:
time: 238 us
  waiting for transfers between devices  97.5 us (41%)
  blocking collectives  72.3 us (30%)
  matrix products  32.6 us (14%)
  between operations  14 us (6%)
  local copies, waits for them, and re-layouts  9.41 us (4%)
  other arithmetic  6.92 us (3%)
  starting transfers between devices  4.68 us (2%)
    all_gather x1, waiting for transfers between devices, expert_half(): lax.all_gather(lax.all_to_all(outgoing, 'ep', split_axis=0, concat_axis=0...  45.6 us
    all_to_all x1, blocking collectives, expert_half(): lax.all_to_all(outgoing, 'ep', split_axis=0, concat_axis=0, tiled=True)  43.2 us
    reduce_scatter x1, waiting for transfers between devices, expert_half(): lax.psum_scatter(jnp.einsum('secf,efd->secd', active, down_proj, preferre...  27.2 us
    all_to_all x1, waiting for transfers between devices, expert_half(): lax.all_to_all(summed, 'ep', split_axis=0, concat_axis=0, tiled=True)  24.6 us
    all_gather x1, blocking collectives, mixer_half(): value_piece = lax.all_gather(projected_values, 'ep', axis=0, tiled=True)  14.8 us
    all_gather x1, blocking collectives, mixer_half(): key_piece = lax.all_gather(keys_turned, 'ep', axis=0, tiled=True)  14.4 us
    dot_general x1, matrix products, expert_half(): jnp.einsum('secf,efd->secd', active, down_proj, preferred_element_type=jn...  11.9 us
    dot_general x1, matrix products, expert_half(): jnp.einsum('secd,edf->secf', rows_in, up_proj, preferred_element_type=jnp...  8.52 us
  transfers between devices with their start and end apart: 4, of which 3 were waited for; matrix products, arithmetic and copies ran while one was open for 9% of the time, Pallas kernels for 0%

commit v1 on v0

--- a/solution.py
+++ b/solution.py
@@ -146,7 +146,18 @@
         scatter_dimension=0,
         tiled=True,
     )
-    returned = lax.all_to_all(summed, "ep", split_axis=0, concat_axis=0, tiled=True)
+    ways, here = (lax.axis_size("ep"), lax.axis_index("ep"))
+    width = summed.shape[0] // ways
+    dims = list(summed.shape)
+    dims[0] = width
+    height = dims[0]
+    dims[0] = height * ways
+    returned = jnp.zeros(dims, summed.dtype)
+    for mask in range(ways):
+        part = lax.dynamic_slice_in_dim(summed, (here ^ mask) * width, width, axis=0)
+        if mask:
+            part = lax.ppermute(part, "ep", [(d, d ^ mask) for d in range(ways)])
+        returned = lax.dynamic_update_slice_in_dim(returned, part, (here ^ mask) * height, axis=0)
     results = returned.reshape(experts_all * capacity, model_dim)
     selected_expert = target.reshape(length, top_count)
     first_weight = jax.nn.sigmoid(expert_score[:, 0] - expert_score[:, 1])

time: 238 us -> 236 us (level); the launches traced: 238 us -> 232 us
  waiting for transfers between devices: 97.5 us -> 86.3 us
  local copies, waits for them, and re-layouts: 9.41 us -> 14.6 us
    ppermute x0 -> x3, waiting for transfers between devices: none -> 26 us  [expert_half(): part = lax.ppermute(part, 'ep', [(d, d ^ mask) for d in range(ways)])]
    all_to_all x1 -> x0, waiting for transfers between devices: 24.6 us -> none  [expert_half(): lax.all_to_all(summed, 'ep', split_axis=0, concat_axis=0, tiled=True)]
    reduce_scatter x1, waiting for transfers between devices: 27.2 us -> 14.7 us  [expert_half(): lax.psum_scatter(jnp.einsum('secf,efd->secd', active, down_proj, preferre...]
    all_to_all x1 -> x0, starting transfers between devices: 4.59 us -> none  [expert_half(): lax.all_to_all(summed, 'ep', split_axis=0, concat_axis=0, tiled=True)]
    ppermute x0 -> x3, starting transfers between devices: none -> 4.45 us  [expert_half(): part = lax.ppermute(part, 'ep', [(d, d ^ mask) for d in range(ways)])]
  transfers between devices with their start and end apart: 4 -> 6, of which waited for: 3 -> 4; matrix products, arithmetic and copies ran while one was open for 9% -> 11% of each run, Pallas kernels for 0% -> 0%
where the time goes in v1:
time: 236 us; the launch traced here: 232 us
  waiting for transfers between devices  86.3 us (37%)
  blocking collectives  72.5 us (31%)
  matrix products  32.7 us (14%)
  local copies, waits for them, and re-layouts  14.6 us (6%)
  between operations  14 us (6%)
  other arithmetic  6.93 us (3%)
  starting transfers between devices  4.57 us (2%)
    all_gather x1, waiting for transfers between devices, expert_half(): lax.all_gather(lax.all_to_all(outgoing, 'ep', split_axis=0, concat_axis=0...  45.6 us
    all_to_all x1, blocking collectives, expert_half(): lax.all_to_all(outgoing, 'ep', split_axis=0, concat_axis=0, tiled=True)  43.2 us
    ppermute x3, waiting for transfers between devices, expert_half(): part = lax.ppermute(part, 'ep', [(d, d ^ mask) for d in range(ways)])  26 us
    all_gather x1, blocking collectives, mixer_half(): value_piece = lax.all_gather(projected_values, 'ep', axis=0, tiled=True)  14.9 us
    reduce_scatter x1, waiting for transfers between devices, expert_half(): lax.psum_scatter(jnp.einsum('secf,efd->secd', active, down_proj, preferre...  14.7 us
    all_gather x1, blocking collectives, mixer_half(): key_piece = lax.all_gather(keys_turned, 'ep', axis=0, tiled=True)  14.4 us
    dot_general x1, matrix products, expert_half(): jnp.einsum('secf,efd->secd', active, down_proj, preferred_element_type=jn...  11.9 us
    dot_general x1, matrix products, expert_half(): jnp.einsum('secd,edf->secf', rows_in, up_proj, preferred_element_type=jnp...  8.52 us
  transfers between devices with their start and end apart: 6, of which 4 were waited for; matrix products, arithmetic and copies ran while one was open for 11% of the time, Pallas kernels for 0%

profile of v1, /device:TPU:0, one launch (start us, length us, event | category | flops | bytes accessed | tf_op | source)
XLA Modules:
  0.0 231.8 jit_solution(18405090323270470741)
XLA Ops:
  7.2 0.9 copy.74
  8.4 1.2 reduce-window.6
  11.1 1.2 fusion.39
  12.3 1.7 convolution_convert_fusion
  14.1 43.2 %all_to_all.5 = bf16[4,1,96,2048]{3,2,1,0:T(8,128)(2,1)} all-to-all(bf16[4,1,96,2048]{3,2,1,0:T(8,128)(2,1)S(1)} %bitcast.174), channel_id=1, replica_groups=mesh['grp'=2,'ep'=4,'tp'=4] {'ep'}, dimensions={0} | all-to-all | bytes 3145728 | tf_op jit(solution)/shard_map/all_to_all | solution.py:133
  57.4 45.6 %all-gather.2.cloned.1.call-done = bf16[16,1,96,2048]{3,2,1,0:T(8,128)(2,1)} async-done(((bf16[4,1,96,2048]{3,2,1,0:T(8,128)(2,1)}), bf16[16,1,96,2048]{3,2,1,0:T(8,128)(2,1)}) %all-gather.2.cloned.1.call-update) | async-done | bytes 6291472 | tf_op jit(solution)/shard_map/all_gather | solution.py:132
  103.0 8.5 %fusion.15 = f32[16,96,512]{2,1,0:T(8,128)} fusion(bf16[16,1,96,2048]{3,2,1,0:T(8,128)(2,1)} %all-gather.2.cloned.1.call-done, bf16[1,2048,512]{2,1,0:T(8,128)(2,1)} %param.26), kind=kOutput, calls=%fused_computation.24 | convolution fusion | flops 3221225472 | bytes 11534336 | tf_op jit(solution)/shard_map/secd,edf->secf/dot_general | solution.py:139
  111.5 11.9 %convert_bitcast_fusion = bf16[16,1,96,2048]{3,2,0,1:T(8,128)(2,1)} fusion(bf16[1,512,2048]{2,1,0:T(8,128)(2,1)S(1)} %copy-done, f32[16,96,512]{2,1,0:T(8,128)} %fusion.15, bf16[1,2048,512]{2,1,0:T(8,128)(2,1)} %param.25, bf16[16,1,96,2048]{3,2,1,0:T(8,128)(2,1)} %all-gather.2.cloned.1.call-done), kind=kOutput, calls=%fused_computation.28 | convolution fusion | flops 6450315264 | bytes 19922944 | tf_op jit(solution)/shard_map/secf,efd->secd/dot_general | solution.py:142
  123.5 0.8 copy-done.2
  126.1 14.4 %all_gather.9 = bf16[768,128]{1,0:T(8,128)(2,1)} all-gather(bf16[192,128]{1,0:T(8,128)(2,1)S(1)} %copy.70), channel_id=1, replica_groups=mesh['grp'=2,'ep'=4,'tp'=4] {'ep'}, dimensions={0}, use_global_device_ids=true | all-gather | bytes 245760 | tf_op jit(solution)/shard_map/all_gather | solution.py:58
  140.5 14.9 %all_gather.10 = bf16[768,128]{1,0:T(8,128)(2,1)} all-gather(bf16[192,128]{1,0:T(8,128)(2,1)S(1)} %copy-done.4), channel_id=1, replica_groups=mesh['grp'=2,'ep'=4,'tp'=4] {'ep'}, dimensions={0}, use_global_device_ids=true | all-gather | bytes 245760 | tf_op jit(solution)/shard_map/all_gather | solution.py:59
  155.4 8.8 %while.18 = (s32[]{:T(128)}, f32[1,4,192]{2,1,0:T(4,128)S(1)}, f32[1,4,192]{2,1,0:T(4,128)S(1)}, f32[192,1,4,128]{3,0,2,1:T(8,128)S(1)}, bf16[768,128]{1,0:T(8,1...) while((s32[]{:T(128)}, f32[1,4,192]{2,1,0:T(4,128)S(1)}, ...), condition=%wide.region_5.6_spmd.clone, body=%wide.region_2.5_spmd.clone.sunk | while | flops 102142472 | bytes 3522735 | solution.py:91
  155.4 1.2 fusion.75
  156.7 1.2 fusion.78
  158.3 1.2 fusion.75
  159.6 1.2 fusion.78
  161.3 1.3 fusion.75
  162.5 1.2 fusion.78
  164.5 3.2 %convolution_convert_fusion.1 = bf16[192,2048]{1,0:T(8,128)(2,1)} fusion(bf16[512,2048]{1,0:T(8,128)(2,1)} %param.20, bf16[24,8,4,128]{3,2,1,0:T(4,128)(2,1)S(1)} %bitcast.179), kind=kOutput, calls=%fused_computation.37 | convolution fusion | flops 403046400 | bytes 3080192 | tf_op jit(solution)/shard_map/dot_general | solution.py:98
  167.8 14.7 %reduce-scatter.5.cloned.1.call-done = bf16[4,1,96,2048]{3,2,0,1:T(8,128)(2,1)} async-done(((bf16[16,1,96,2048]{3,2,0,1:T(8,128)(2,1)}), bf16[4,1,96,2048]{3,2,0,1:T(8,128)(2,1)}) %reduce-scatter.5.cloned.1.call-update) | async-done | bytes 1572880 | tf_op jit(solution)/shard_map/reduce_scatter | solution.py:141
  182.4 1.3 broadcast_in_dim.15
  184.4 0.9 constant_dynamic-slice_fusion
  185.3 1.5 collective-permute-start
  186.8 2.4 %collective-permute-start.1 = (bf16[1,1,96,2048]{3,2,0,1:T(8,128)(2,1)S(1)}, bf16[1,1,96,2048]{3,2,0,1:T(8,128)(2,1)S(1)}, u32[]{:S(2)}, u32[]{:S(2)}) collective-permute-start(bf16[1,1,96,2048]{3,2,0,1:T(8,128)(2,1)S(1)} %get-tuple-element.209), channel_id=1, source_target_pairs={{0,8},{4,12},{8,0},{12,4},{1,9},{5,13},{9,1},{13,5},{2,10},{6,14},... | collective-permute-start | bytes 1179656 | tf_op jit(solution)/shard_map/ppermute | solution.py:159
  189.8 13.7 %collective-permute-done = bf16[1,1,96,2048]{3,2,0,1:T(8,128)(2,1)S(1)} collective-permute-done((bf16[1,1,96,2048]{3,2,0,1:T(8,128)(2,1)S(1)}, bf16[1,1,96,2048]{3,2,0,1:T(8,128)(2,1)S(1)}, u32[]{:S(2)}, u32[]{:S(2)}) %collective-permute-start) | collective-permute-done | bytes 393248 | tf_op jit(solution)/shard_map/ppermute | solution.py:159
  203.5 0.8 constant_dynamic-update-slice_fusion.1
  204.3 12.2 %collective-permute-done.1 = bf16[1,1,96,2048]{3,2,0,1:T(8,128)(2,1)S(1)} collective-permute-done((bf16[1,1,96,2048]{3,2,0,1:T(8,128)(2,1)S(1)}, bf16[1,1,96,2048]{3,2,0,1:T(8,128)(2,1)S(1)}, u32[]{:S(2)}, u32[]{:S(2)}) %collective-permute-start.1) | collective-permute-done | bytes 393248 | tf_op jit(solution)/shard_map/ppermute | solution.py:159
  216.6 0.8 constant_dynamic-update-slice_fusion
  217.3 0.8 constant_dynamic-update-slice_fusion.2
  218.1 3.0 %gather_fusion = bf16[128,2048]{1,0:T(8,128)(2,1)S(1)} fusion(bf16[384,2048]{1,0:T(8,128)(2,1)} %bitcast.33, s32[1024]{0:T(1024)S(1)} %get-tuple-element.229), kind=kCustom, calls=%fused_computation | custom fusion | bytes 1049088 | tf_op jit(solution)/shard_map/gather | solution.py:164
  221.2 3.1 %gather_fusion.1 = bf16[128,2048]{1,0:T(8,128)(2,1)S(1)} fusion(bf16[384,2048]{1,0:T(8,128)(2,1)} %bitcast.33, s32[1024]{0:T(1024)S(1)} %get-tuple-element.228), kind=kCustom, calls=%fused_computation.1 | custom fusion | bytes 1049088 | tf_op jit(solution)/shard_map/gather | solution.py:166
  224.3 1.0 add_convert_fusion
  (78 shorter events, 6.3 us)
Async XLA Ops:
  7.2 104.3 %copy-start = (bf16[1,512,2048]{2,1,0:T(8,128)(2,1)S(1)}, bf16[1,512,2048]{2,1,0:T(8,128)(2,1)}, u32[]{:S(2)}) copy-start(bf16[1,512,2048]{2,1,0:T(8,128)(2,1)} %param.27) | copy-start | bytes 6291460
  7.2 95.8 %all-gather.2.cloned.1.call-start = ((), (), s32[]{:S(2)}) async-start(), calls=%async_computation.4 | async-start | bytes 7864320 | tf_op jit(solution)/shard_map/all_gather | solution.py:132
  57.3 125.1 %reduce-scatter.5.cloned.1.call-start = ((), (), s32[]{:S(2)}) async-start(), calls=%async_computation.5 | async-start | bytes 7864320 | tf_op jit(solution)/shard_map/reduce_scatter | solution.py:141
  123.4 0.9 copy-start.2
  123.4 1.1 copy-start.7
  123.4 2.0 copy-start.3
  123.4 2.2 copy-start.6
  123.5 101.8 %reduce-scatter.3.cloned.1.call-start = ((), (), s32[]{:S(2)}) async-start(), calls=%async_computation.3 | async-start | bytes 983040 | tf_op jit(solution)/shard_map/reduce_scatter | solution.py:97
  124.9 15.6 %copy-start.4 = (bf16[192,128]{1,0:T(8,128)(2,1)S(1)}, bf16[192,128]{1,0:T(8,128)(2,1)}, u32[]{:S(2)}) copy-start(bf16[192,128]{1,0:T(8,128)(2,1)} %param.17) | copy-start | bytes 147460
  182.4 2.0 copy-start.1
  182.4 6.8 %copy-start.5 = (f32[128,2]{0,1:T(2,128)S(1)}, f32[128,2]{0,1:T(2,128)}, u32[]{:S(2)}) copy-start(f32[128,2]{0,1:T(2,128)} %param.24) | copy-start | bytes 3076
  185.3 18.2 %collective-permute-start = (bf16[1,1,96,2048]{3,2,0,1:T(8,128)(2,1)S(1)}, bf16[1,1,96,2048]{3,2,0,1:T(8,128)(2,1)S(1)}, u32[]{:S(2)}, u32[]{:S(2)}) collective-permute-start(bf16[1,1,96,2048]{3,2,0,1:T(8,128)(2,1)S(1)} %get-tuple-element.210), channel_id=1, source_target_pairs={{0,4},{4,0},{8,12},{12,8},{1,5},{5,1},{9,13},{13,9},{2,6},{6,2},{1... | collective-permute-start | bytes 1179656 | tf_op jit(solution)/shard_map/ppermute | solution.py:159
  186.8 29.7 %collective-permute-start.1 = (bf16[1,1,96,2048]{3,2,0,1:T(8,128)(2,1)S(1)}, bf16[1,1,96,2048]{3,2,0,1:T(8,128)(2,1)S(1)}, u32[]{:S(2)}, u32[]{:S(2)}) collective-permute-start(bf16[1,1,96,2048]{3,2,0,1:T(8,128)(2,1)S(1)} %get-tuple-element.209), channel_id=1, source_target_pairs={{0,8},{4,12},{8,0},{12,4},{1,9},{5,13},{9,1},{13,5},{2,10},{6,14},... | collective-permute-start | bytes 1179656 | tf_op jit(solution)/shard_map/ppermute | solution.py:159
  189.3 28.1 %collective-permute-start.2 = (bf16[1,1,96,2048]{3,2,0,1:T(8,128)(2,1)S(1)}, bf16[1,1,96,2048]{3,2,0,1:T(8,128)(2,1)S(1)}, u32[]{:S(2)}, u32[]{:S(2)}) collective-permute-start(bf16[1,1,96,2048]{3,2,0,1:T(8,128)(2,1)S(1)} %get-tuple-element.208), channel_id=1, source_target_pairs={{0,12},{4,8},{8,4},{12,0},{1,13},{5,9},{9,5},{13,1},{2,14},{6,10},... | collective-permute-start | bytes 1179656 | tf_op jit(solution)/shard_map/ppermute | solution.py:159
Sparse Core Ops, SparseCore 0:
  57.4 45.4 all-gather.1
  123.5 58.8 reduce-scatter.4
  185.5 23.2 reduce-scatter.2
